TPU v7x, 32 devices: a whole 2x2x4 slice. The times are simulated.
32 devices in a mesh: grp: 2 (over y), dp: 2 (over x), kv: 4 (over z), tp: 2 (over core).
Axes of the slice: x: 2, y: 2, z: 4, core: 2. Of those that a mesh axis runs over, the one named last changes fastest.
Arguments:
- tokens: bfloat16 [32, 2048], P(('grp', 'dp'), ('kv', 'tp')), parts along dimension 0, may hold values from -24 to 24
- memory: float32 [32, 12, 16384], P(('grp', 'dp', 'kv', 'tp')), parts along dimension 0, may hold values from -3 to 3
- mix_gain: float32 [2048], replicated, may hold values from 0.1 to 1.9
- w_query: bfloat16 [2048, 1536], P(None, ('kv', 'tp')), may hold values from -0.125 to 0.125
- w_key: bfloat16 [2048, 1536], P(None, ('kv', 'tp')), may hold values from -0.125 to 0.125
- w_value: bfloat16 [2048, 1536], P(None, ('kv', 'tp')), may hold values from -0.125 to 0.125
- w_gate: bfloat16 [2048, 1536], P(None, ('kv', 'tp')), may hold values from -0.125 to 0.125
- w_beta: bfloat16 [2048, 12], replicated, may hold values from -0.125 to 0.125
- w_decay: bfloat16 [2048, 12], replicated, may hold values from -0.125 to 0.125
- decay_rate: float32 [12], replicated, may hold values from 0.1 to 3
- decay_bias: float32 [12], replicated, may hold values from -2 to 1
- head_gain: float32 [128], replicated, may hold values from 0.1 to 1.9
- w_out: bfloat16 [1536, 2048], P(None, ('kv', 'tp')), may hold values from -0.15625 to 0.15625
- ffn_gain: float32 [2048], replicated, may hold values from 0.1 to 1.9
- w_up: bfloat16 [2048, 8192], P(None, ('kv', 'tp')), may hold values from -0.125 to 0.125
- w_down: bfloat16 [8192, 2048], P(('kv', 'tp')), may hold values from -0.09375 to 0.09375
Outputs:
- layer_out: bfloat16 [32, 2048], P(('grp', 'dp'), ('kv', 'tp')), parts along dimension 0
- new_memory: float32 [32, 12, 16384], P(('grp', 'dp', 'kv', 'tp')), parts along dimension 0
There are 2 independent parts, one for each index of `grp`. A program takes and returns all parts, laid end to end along the dimension named above; an argument that names none is the same for every part. Nothing has to cross between parts.
All inputs are finite; a program needn't handle non-finite values.
Results may differ from a plain program's by a relative error of at most 0.02.
Values may be sent and summed in bfloat16 or wider, within the bound.
A program may use at most 64 MiB of HBM per device.

v0:
```python
import jax
import jax.numpy as jnp
from jax import lax
from jax.sharding import PartitionSpec as P

epsilon = 1e-06


def shortened(value):
    return jax.tree.map(lambda a: a.astype(jnp.bfloat16) if a.dtype == jnp.float32 else a, value)


def delta_step(queries, keys_in, values, gates, strength, log_decay, memory, head_gain):
    count = queries.shape[0]
    heads = strength.shape[1]
    size = head_gain.shape[0]
    highest = lax.Precision.HIGHEST
    query_wide = queries.astype(jnp.float32).reshape(count, heads, size)
    key_wide = keys_in.astype(jnp.float32).reshape(count, heads, size)
    value_wide = values.astype(jnp.float32).reshape(count, heads, size)
    gate_wide = gates.astype(jnp.float32).reshape(count, heads, size)
    unit_key = key_wide * lax.rsqrt(jnp.sum(key_wide * key_wide, axis=-1, keepdims=True) + epsilon)
    matrix = memory.reshape(count, heads, size, size)
    recall = jnp.einsum("bhk,bhkv->bhv", unit_key, matrix, precision=highest)
    retain = jnp.exp(log_decay)[:, :, None, None]
    scaled = strength[:, :, None]
    erased = matrix - jnp.einsum("bhk,bhv->bhkv", unit_key, scaled * recall, precision=highest)
    written = jnp.einsum("bhk,bhv->bhkv", unit_key, scaled * value_wide, precision=highest)
    updated = retain * erased + written
    readout = jnp.einsum("bhk,bhkv->bhv", query_wide, updated, precision=highest)
    normed = readout * lax.rsqrt(jnp.mean(readout * readout, axis=-1, keepdims=True) + epsilon)
    normed = normed * head_gain * jax.nn.silu(gate_wide)
    return (
        updated.reshape(count, heads, size * size),
        normed.reshape(count, heads * size).astype(jnp.bfloat16),
    )


def per_device(
    tokens,
    memory,
    mix_gain,
    w_query,
    w_key,
    w_value,
    w_gate,
    w_beta,
    w_decay,
    decay_rate,
    decay_bias,
    head_gain,
    w_out,
    ffn_gain,
    w_up,
    w_down,
):
    rows = tokens.shape[0]
    owned = memory.shape[0]
    width = mix_gain.shape[0]
    lane = lax.axis_index(("kv", "tp"))
    own_start = lane * owned
    wide = tokens.astype(jnp.float32)
    head_weights = (w_query, w_key, w_value, w_gate)
    small_weights = (w_beta, w_decay)

    def fold_proj(carry, piece, start):
        mine = lax.dynamic_slice_in_dim(piece, own_start, owned, 0)
        large = tuple(
            (jnp.dot(piece, weight, preferred_element_type=jnp.float32) for weight in head_weights)
        )
        small = tuple(
            (jnp.dot(mine, weight, preferred_element_type=jnp.float32) for weight in small_weights)
        )
        return large + small

    def fold_up(total, piece, start):
        return jnp.dot(piece, w_up, preferred_element_type=jnp.float32)

    def with_squares(inner, gain, carry, piece, start):
        piece_wide = piece.astype(jnp.float32)
        lifted = (piece_wide * gain).astype(jnp.bfloat16)
        return (inner(carry[0], lifted, start), jnp.sum(piece_wide * piece_wide, axis=1))

    proj_init = tuple((jnp.zeros((rows, weight.shape[1]), jnp.float32) for weight in head_weights))
    proj_init = proj_init + tuple(
        (jnp.zeros((owned, weight.shape[1]), jnp.float32) for weight in small_weights)
    )
    row_zeros = jnp.zeros((rows,), jnp.float32)
    folded, total_in = with_squares(
        fold_proj,
        mix_gain,
        (proj_init, row_zeros),
        lax.all_gather(tokens, ("kv", "tp"), axis=1, tiled=True),
        jnp.int32(0),
    )
    scale_in = lax.rsqrt(total_in / width + epsilon)
    sent = tuple(((total * scale_in[:, None]).astype(jnp.bfloat16) for total in folded[:4]))
    scale_own = lax.dynamic_slice_in_dim(scale_in, own_start, owned)[:, None]
    strength = jax.nn.sigmoid(folded[4] * scale_own)
    log_decay = -decay_rate * jax.nn.softplus(folded[5] * scale_own + decay_bias)
    queries, keys_in, values, gates = jax.tree.map(
        lambda part, own: part.astype(own.dtype),
        lax.all_to_all(shortened(sent), ("kv", "tp"), split_axis=0, concat_axis=1, tiled=True),
        sent,
    )
    updated, mixed = delta_step(
        queries, keys_in, values, gates, strength, log_decay, memory, head_gain
    )
    branch = jnp.dot(
        lax.all_gather(mixed, ("kv", "tp"), axis=0, tiled=True),
        w_out,
        preferred_element_type=jnp.float32,
    )
    middle = (wide + branch).astype(jnp.bfloat16)
    middle_wide = middle.astype(jnp.float32)
    up_init = jnp.zeros((rows, w_up.shape[1]), jnp.float32)
    raised, total_mid = with_squares(
        fold_up,
        ffn_gain,
        (up_init, row_zeros),
        lax.all_gather(middle, ("kv", "tp"), axis=1, tiled=True),
        jnp.int32(0),
    )
    scale_mid = lax.rsqrt(total_mid / width + epsilon)[:, None]
    hidden = jnp.square(jax.nn.relu(raised * scale_mid)).astype(jnp.bfloat16)
    terms = jnp.dot(hidden, w_down, preferred_element_type=jnp.float32)
    down = lax.psum_scatter(
        terms.astype(jnp.bfloat16), ("kv", "tp"), scatter_dimension=1, tiled=True
    ).astype(jnp.float32)
    layer_out = (middle_wide + down).astype(jnp.bfloat16)
    return (layer_out, updated)


def solution(mesh):
    placed = (
        P(("grp", "dp"), ("kv", "tp")),
        P(("grp", "dp", "kv", "tp"), None, None),
        P(),
        P(None, ("kv", "tp")),
        P(None, ("kv", "tp")),
        P(None, ("kv", "tp")),
        P(None, ("kv", "tp")),
        P(),
        P(),
        P(),
        P(),
        P(),
        P(None, ("kv", "tp")),
        P(),
        P(None, ("kv", "tp")),
        P(("kv", "tp"), None),
    )
    return jax.shard_map(
        per_device,
        mesh=mesh,
        in_specs=placed,
        out_specs=(P(("grp", "dp"), ("kv", "tp")), P(("grp", "dp", "kv", "tp"), None, None)),
        check_vma=False,
    )
```

profile of v0, /device:TPU:0, one launch (start us, length us, event | category | flops | bytes accessed | tf_op | source)
XLA Modules:
  0.0 142.1 jit_solution(9691909267525715545)
XLA Ops:
  7.2 0.0 copy-start
  7.2 0.0 copy-start.3
  7.2 16.1 %all_gather.9 = bf16[8,2048]{1,0:T(8,128)(2,1)S(1)} all-gather(bf16[8,256]{1,0:T(8,128)(2,1)} %param.16), channel_id=1, replica_groups=mesh['grp'=2,'dp'=2,'kv'=4,'tp'=2] {'kv','tp'}, dimensions={1}, use_global_device_ids=true | all-gather | bytes 36864 | tf_op jit(solution)/shard_map/all_gather | solution.py:93
  23.3 0.8 fusion.20
  24.1 1.4 %fusion.10 = bf16[8,1,192]{2,0,1:T(8,128)(2,1)S(1)} fusion(bf16[8,2048]{1,0:T(8,128)(2,1)S(1)} %get-tuple-element.5, bf16[2048,192]{0,1:T(8,128)(2,1)} %param.20, f32[8]{0:T(128)S(1)} %add_rsqrt_fusion.3), kind=kOutput, calls=%fused_computation.17 | convolution fusion | flops 6294528 | bytes 822304 | tf_op jit(solution)/shard_map/dot_general | solution.py:69
  25.6 0.6 copy.23
  26.2 4.6 %all-to-all-start.1 = ((bf16[8,1,192]{2,1,0:T(2,128)(2,1)}), bf16[8,1,192]{2,1,0:T(2,128)(2,1)S(1)}, u32[]{:S(2)}, u32[]{:S(2)}) async-start(bf16[8,1,192]{2,1,0:T(2,128)(2,1)} %copy.23), calls=%async_computation.1 | async-start | bytes 16384 | tf_op jit(solution)/shard_map/all_to_all | solution.py:103
  30.8 0.6 dynamic_slice.7
  31.4 1.4 %fusion.9 = bf16[8,1,192]{2,0,1:T(8,128)(2,1)S(1)} fusion(bf16[8,2048]{1,0:T(8,128)(2,1)S(1)} %get-tuple-element.5, bf16[2048,192]{0,1:T(8,128)(2,1)} %param.21, f32[8]{0:T(128)S(1)} %add_rsqrt_fusion.3), kind=kOutput, calls=%fused_computation.16 | convolution fusion | flops 6294528 | bytes 822304 | tf_op jit(solution)/shard_map/dot_general | solution.py:69
  32.8 1.5 %fusion.8 = bf16[8,1,192]{2,0,1:T(8,128)(2,1)S(1)} fusion(bf16[8,2048]{1,0:T(8,128)(2,1)S(1)} %get-tuple-element.5, bf16[2048,192]{0,1:T(8,128)(2,1)} %param.22, f32[8]{0:T(128)S(1)} %add_rsqrt_fusion.3), kind=kOutput, calls=%fused_computation.15 | convolution fusion | flops 6294528 | bytes 822304 | tf_op jit(solution)/shard_map/dot_general | solution.py:69
  34.3 1.6 %fusion.16 = f32[12]{0:T(128)S(1)} fusion(bf16[2048,12]{0,1:T(8,128)(2,1)} %param.23, bf16[8,2048]{1,0:T(8,128)(2,1)S(1)} %get-tuple-element.5, s32[]{:T(128)S(6)} %select_n.9, f32[]{:T(128)} %bitcast.2), kind=kOutput, calls=%fused_computation.24 | convolution fusion | flops 49200 | bytes 57400 | tf_op jit(solution)/shard_map/dot_general | solution.py:72
  35.9 1.7 %fusion.45 = f32[12]{0:T(128)S(1)} fusion(f32[12]{0:T(128)} %param.26, bf16[2048,12]{0,1:T(8,128)(2,1)} %param.24, bf16[8,2048]{1,0:T(8,128)(2,1)S(1)} %get-tuple-element.5, s32[]{:T(128)S(6)} %select_n.9, f32[12]{0:T(128)} %param.25, f32[]{:T(128)} %bitcast.2), kind=kOutput, calls=%fused_computation.68 | convolution fusion | flops 49272 | bytes 57496 | tf_op jit(solution)/shard_map/dot_general | solution.py:72
  37.6 1.5 %fusion.11 = bf16[8,1,192]{2,0,1:T(8,128)(2,1)S(1)} fusion(bf16[8,2048]{1,0:T(8,128)(2,1)S(1)} %get-tuple-element.5, bf16[2048,192]{0,1:T(8,128)(2,1)} %param.19, f32[8]{0:T(128)S(1)} %add_rsqrt_fusion.3), kind=kOutput, calls=%fused_computation.18 | convolution fusion | flops 6294528 | bytes 822304 | tf_op jit(solution)/shard_map/dot_general | solution.py:69
  39.0 0.6 copy.24
  39.7 0.6 copy.22
  40.3 0.6 copy.25
  40.9 0.0 all-to-all-done.1
  40.9 5.1 %all-to-all-start.3 = ((bf16[8,1,192]{2,1,0:T(2,128)(2,1)}), bf16[8,1,192]{2,1,0:T(2,128)(2,1)S(1)}, u32[]{:S(2)}, u32[]{:S(2)}) async-start(bf16[8,1,192]{2,1,0:T(2,128)(2,1)} %copy.25), calls=%async_computation.3 | async-start | bytes 16384 | tf_op jit(solution)/shard_map/all_to_all | solution.py:103
  46.0 0.1 mul.179
  46.1 0.1 reduce_sum.37
  46.2 0.1 reshape.229
  46.3 0.1 fusion.68
  46.4 5.2 %all-to-all-done.3 = bf16[8,1,192]{2,1,0:T(2,128)(2,1)S(1)} async-done(((bf16[8,1,192]{2,1,0:T(2,128)(2,1)}), bf16[8,1,192]{2,1,0:T(2,128)(2,1)S(1)}, u32[]{:S(2)}, u32[]{:S(2)}) %all-to-all-start.3) | async-done | bytes 3104 | tf_op jit(solution)/shard_map/all_to_all | solution.py:103
  51.6 3.3 %all-to-all-start = ((bf16[8,1,192]{2,1,0:T(2,128)(2,1)}), bf16[8,1,192]{2,1,0:T(2,128)(2,1)S(1)}, u32[]{:S(2)}, u32[]{:S(2)}) async-start(bf16[8,1,192]{2,1,0:T(2,128)(2,1)} %copy.22), calls=%async_computation | async-start | bytes 16384 | tf_op jit(solution)/shard_map/all_to_all | solution.py:103
  54.9 0.1 broadcast_multiply_fusion.1
  55.0 5.5 %all-to-all-done = bf16[8,1,192]{2,1,0:T(2,128)(2,1)S(1)} async-done(((bf16[8,1,192]{2,1,0:T(2,128)(2,1)}), bf16[8,1,192]{2,1,0:T(2,128)(2,1)S(1)}, u32[]{:S(2)}, u32[]{:S(2)}) %all-to-all-start) | async-done | bytes 3104 | tf_op jit(solution)/shard_map/all_to_all | solution.py:103
  60.5 3.3 %all-to-all-start.2 = ((bf16[8,1,192]{2,1,0:T(2,128)(2,1)}), bf16[8,1,192]{2,1,0:T(2,128)(2,1)S(1)}, u32[]{:S(2)}, u32[]{:S(2)}) async-start(bf16[8,1,192]{2,1,0:T(2,128)(2,1)} %copy.24), calls=%async_computation.2 | async-start | bytes 16384 | tf_op jit(solution)/shard_map/all_to_all | solution.py:103
  63.8 0.0 reduce-scatter.2.cloned.1.call-start
  63.9 0.1 reshape.231
  64.0 0.1 reshape.244
  64.1 5.3 %all-to-all-done.2 = bf16[8,1,192]{2,1,0:T(2,128)(2,1)S(1)} async-done(((bf16[8,1,192]{2,1,0:T(2,128)(2,1)}), bf16[8,1,192]{2,1,0:T(2,128)(2,1)S(1)}, u32[]{:S(2)}, u32[]{:S(2)}) %all-to-all-start.2) | async-done | bytes 3104 | tf_op jit(solution)/shard_map/all_to_all | solution.py:103
  69.4 0.1 reshape.230
  69.5 0.8 fusion.38
  70.2 0.1 bitcast_multiply_fusion.2
  70.3 0.3 multiply_add_fusion
  70.6 0.0 copy-start.2
  70.6 0.5 fusion.51
  71.1 0.1 fusion.33
  71.2 0.1 fusion.36
  71.3 14.0 %all-gather = bf16[8,1,1536]{2,1,0:T(2,128)(2,1)S(1)} all-gather(bf16[1,1,1536]{2,1,0:T(2,128)(2,1)S(1)} %reshape.232), channel_id=1, replica_groups=mesh['grp'=2,'dp'=2,'kv'=4,'tp'=2] {'kv','tp'}, dimensions={0}, use_global_device_ids=true | all-gather | bytes 27648 | tf_op jit(solution)/shard_map/all_gather | solution.py:110
  85.3 0.0 copy-done
  85.3 0.2 fusion.7
  85.5 14.1 %all_gather.11 = bf16[8,2048]{1,0:T(8,128)(2,1)S(1)} all-gather(bf16[8,256]{1,0:T(8,128)(2,1)S(1)} %fusion.7), channel_id=1, replica_groups=mesh['grp'=2,'dp'=2,'kv'=4,'tp'=2] {'kv','tp'}, dimensions={1}, use_global_device_ids=true | all-gather | bytes 36864 | tf_op jit(solution)/shard_map/all_gather | solution.py:121
  99.6 0.1 fusion.22
  99.8 5.3 %convolution_convert_fusion = bf16[8,2048]{1,0:T(8,128)(2,1)} fusion(bf16[1024,2048]{1,0:T(8,128)(2,1)} %param.31, bf16[2048,1024]{1,0:T(8,128)(2,1)} %param.30, bf16[8,2048]{1,0:T(8,128)(2,1)S(1)} %all_gather.11, f32[2048]{0:T(1024)S(1)} %copy-done.4, f32[8]{0:T(128)S(1)} %add_rsqrt_fusion), kind=kOutput, calls=%fused_computation | convolution fusion | flops 67207168 | bytes 8462368 | tf_op jit(solution)/shard_map/dot_general | solution.py:126
  105.1 0.0 reduce-scatter.2.cloned.1.call-update
  105.1 28.9 %reduce-scatter.2.cloned.1.call-done = bf16[8,256]{1,0:T(8,128)(2,1)} async-done(((bf16[8,2048]{1,0:T(8,128)(2,1)}), bf16[8,256]{1,0:T(8,128)(2,1)}) %reduce-scatter.2.cloned.1.call-update) | async-done | bytes 4112 | tf_op jit(solution)/shard_map/reduce_scatter | solution.py:127
  134.0 1.3 add_convert_fusion
  (17 shorter events, 0.2 us)
Async XLA Ops:
  7.2 78.2 %copy-start = (bf16[1536,256]{1,0:T(8,128)(2,1)S(1)}, bf16[1536,256]{1,0:T(8,128)(2,1)}, u32[]{:S(2)}) copy-start(bf16[1536,256]{1,0:T(8,128)(2,1)} %param.28) | copy-start | bytes 2359300
  7.2 78.2 %copy-start.3 = (bf16[8,256]{1,0:T(8,128)(2,1)S(1)}, bf16[8,256]{1,0:T(8,128)(2,1)}, u32[]{:S(2)}) copy-start(bf16[8,256]{1,0:T(8,128)(2,1)} %param.16) | copy-start | bytes 12292
  7.2 62.3 %copy-start.1 = (f32[1,12,16384]{2,0,1:T(1,128)S(1)}, f32[1,12,16384]{2,0,1:T(1,128)}, u32[]{:S(2)}) copy-start(f32[1,12,16384]{2,0,1:T(1,128)} %param.17) | copy-start | bytes 2359300
  7.2 64.0 %copy-start.5 = (f32[128]{0:T(128)S(1)}, f32[128]{0:T(128)}, u32[]{:S(2)}) copy-start(f32[128]{0:T(128)} %param.27) | copy-start | bytes 1540
  7.2 92.6 %copy-start.4 = (f32[2048]{0:T(1024)S(1)}, f32[2048]{0:T(1024)}, u32[]{:S(2)}) copy-start(f32[2048]{0:T(1024)} %param.29) | copy-start | bytes 24580
  26.2 14.7 %all-to-all-start.1 = ((bf16[8,1,192]{2,1,0:T(2,128)(2,1)}), bf16[8,1,192]{2,1,0:T(2,128)(2,1)S(1)}, u32[]{:S(2)}, u32[]{:S(2)}) async-start(bf16[8,1,192]{2,1,0:T(2,128)(2,1)} %copy.23), calls=%async_computation.1 | async-start | bytes 16384 | tf_op jit(solution)/shard_map/all_to_all | solution.py:103
  40.9 10.7 %all-to-all-start.3 = ((bf16[8,1,192]{2,1,0:T(2,128)(2,1)}), bf16[8,1,192]{2,1,0:T(2,128)(2,1)S(1)}, u32[]{:S(2)}, u32[]{:S(2)}) async-start(bf16[8,1,192]{2,1,0:T(2,128)(2,1)} %copy.25), calls=%async_computation.3 | async-start | bytes 16384 | tf_op jit(solution)/shard_map/all_to_all | solution.py:103
  51.6 8.9 %all-to-all-start = ((bf16[8,1,192]{2,1,0:T(2,128)(2,1)}), bf16[8,1,192]{2,1,0:T(2,128)(2,1)S(1)}, u32[]{:S(2)}, u32[]{:S(2)}) async-start(bf16[8,1,192]{2,1,0:T(2,128)(2,1)} %copy.22), calls=%async_computation | async-start | bytes 16384 | tf_op jit(solution)/shard_map/all_to_all | solution.py:103
  60.5 8.9 %all-to-all-start.2 = ((bf16[8,1,192]{2,1,0:T(2,128)(2,1)}), bf16[8,1,192]{2,1,0:T(2,128)(2,1)S(1)}, u32[]{:S(2)}, u32[]{:S(2)}) async-start(bf16[8,1,192]{2,1,0:T(2,128)(2,1)} %copy.24), calls=%async_computation.2 | async-start | bytes 16384 | tf_op jit(solution)/shard_map/all_to_all | solution.py:103
  63.8 70.2 %reduce-scatter.2.cloned.1.call-start = ((), (), s32[]{:S(2)}) async-start(), calls=%async_computation.5 | async-start | bytes 36864 | tf_op jit(solution)/shard_map/reduce_scatter | solution.py:127
  70.6 34.5 %copy-start.2 = (f32[12,128,128]{2,1,0:T(8,128)}, f32[12,128,128]{2,1,0:T(8,128)S(1)}, u32[]{:S(2)}) copy-start(f32[12,128,128]{2,1,0:T(8,128)S(1)} %multiply_add_fusion) | copy-start | bytes 2359300
Sparse Core Ops, SparseCore 0:
  105.2 28.7 reduce-scatter.1
where the time goes:
time: 143 us; the launch traced here: 142 us
  waiting for transfers between devices  44.9 us (31%)
  blocking collectives  44.2 us (31%)
  starting transfers between devices  16.4 us (11%)
  matrix products  15.8 us (11%)
  between operations  14.2 us (10%)
  local copies, waits for them, and re-layouts  3.45 us (2%)
  other arithmetic  3.2 us (2%)
    reduce_scatter x1, waiting for transfers between devices, per_device(): lax.psum_scatter(terms.astype(jnp.bfloat16), ('kv', 'tp'), scatter_dimens...  28.9 us
    all_to_all x4, starting transfers between devices, per_device(): lax.all_to_all(shortened(sent), ('kv', 'tp'), split_axis=0, concat_axis=1...  16.4 us
    all_gather x1, blocking collectives, per_device(): lax.all_gather(tokens, ('kv', 'tp'), axis=1, tiled=True)  16.1 us
    all_to_all x4, waiting for transfers between devices, per_device(): lax.all_to_all(shortened(sent), ('kv', 'tp'), split_axis=0, concat_axis=1...  15.9 us
    all_gather x1, blocking collectives, per_device(): lax.all_gather(middle, ('kv', 'tp'), axis=1, tiled=True)  14.1 us
    all_gather x1, blocking collectives, per_device(): lax.all_gather(mixed, ('kv', 'tp'), axis=0, tiled=True)  14 us
    dot_general x4, matrix products, fold_proj(): jnp.dot(piece, weight, preferred_element_type=jnp.float32)  5.79 us
    dot_general x1, matrix products, per_device(): terms = jnp.dot(hidden, w_down, preferred_element_type=jnp.float32)  5.28 us
  transfers between devices with their start and end apart: 5, of which 4 were waited for; matrix products, arithmetic and copies ran while one was open for 8% of the time, Pallas kernels for 0%

commit v1 on v0

--- a/solution.py
+++ b/solution.py
@@ -114,12 +114,13 @@
     middle = (wide + branch).astype(jnp.bfloat16)
     middle_wide = middle.astype(jnp.float32)
     up_init = jnp.zeros((rows, w_up.shape[1]), jnp.float32)
+
+    def create_rates(field):
+        v1 = lax.all_gather(field, ("kv", "tp"))
+        return jnp.concatenate(v1, axis=1)
+
     raised, total_mid = with_squares(
-        fold_up,
-        ffn_gain,
-        (up_init, row_zeros),
-        lax.all_gather(middle, ("kv", "tp"), axis=1, tiled=True),
-        jnp.int32(0),
+        fold_up, ffn_gain, (up_init, row_zeros), create_rates(middle), jnp.int32(0)
     )
     scale_mid = lax.rsqrt(total_mid / width + epsilon)[:, None]
     hidden = jnp.square(jax.nn.relu(raised * scale_mid)).astype(jnp.bfloat16)

time: 143 us -> 143 us (level)
  no operation moved by 1% of the time
where the time goes in v1:
time: 143 us; the launch traced here: 142 us
  waiting for transfers between devices  44.9 us (31%)
  blocking collectives  44.2 us (31%)
  starting transfers between devices  16.4 us (11%)
  matrix products  15.8 us (11%)
  between operations  14.2 us (10%)
  local copies, waits for them, and re-layouts  3.45 us (2%)
  other arithmetic  3.21 us (2%)
    reduce_scatter x1, waiting for transfers between devices, per_device(): lax.psum_scatter(terms.astype(jnp.bfloat16), ('kv', 'tp'), scatter_dimens...  28.9 us
    all_to_all x4, starting transfers between devices, per_device(): lax.all_to_all(shortened(sent), ('kv', 'tp'), split_axis=0, concat_axis=1...  16.4 us
    all_gather x1, blocking collectives, per_device(): lax.all_gather(tokens, ('kv', 'tp'), axis=1, tiled=True)  16.1 us
    all_to_all x4, waiting for transfers between devices, per_device(): lax.all_to_all(shortened(sent), ('kv', 'tp'), split_axis=0, concat_axis=1...  15.9 us
    all_gather x1, blocking collectives, create_rates(): v1 = lax.all_gather(field, ('kv', 'tp'))  14.1 us
    all_gather x1, blocking collectives, per_device(): lax.all_gather(mixed, ('kv', 'tp'), axis=0, tiled=True)  14 us
    dot_general x4, matrix products, fold_proj(): jnp.dot(piece, weight, preferred_element_type=jnp.float32)  5.79 us
    dot_general x1, matrix products, per_device(): terms = jnp.dot(hidden, w_down, preferred_element_type=jnp.float32)  5.28 us
  transfers between devices with their start and end apart: 5, of which 4 were waited for; matrix products, arithmetic and copies ran while one was open for 8% of the time, Pallas kernels for 0%

profile of v1, /device:TPU:0, one launch (start us, length us, event | category | flops | bytes accessed | tf_op | source)
XLA Modules:
  0.0 142.1 jit_solution(15900982767679141224)
XLA Ops:
  7.2 0.0 copy-start
  7.2 16.1 %all_gather.12 = bf16[8,2048]{1,0:T(8,128)(2,1)S(1)} all-gather(bf16[8,256]{1,0:T(8,128)(2,1)} %param.16), channel_id=1, replica_groups=mesh['grp'=2,'dp'=2,'kv'=4,'tp'=2] {'kv','tp'}, dimensions={1}, use_global_device_ids=true | all-gather | bytes 36864 | tf_op jit(solution)/shard_map/all_gather | solution.py:93
  23.3 0.8 fusion.20
  24.1 1.4 %fusion.10 = bf16[8,1,192]{2,0,1:T(8,128)(2,1)S(1)} fusion(bf16[8,2048]{1,0:T(8,128)(2,1)S(1)} %get-tuple-element.5, bf16[2048,192]{0,1:T(8,128)(2,1)} %param.20, f32[8]{0:T(128)S(1)} %add_rsqrt_fusion.3), kind=kOutput, calls=%fused_computation.17 | convolution fusion | flops 6294528 | bytes 822304 | tf_op jit(solution)/shard_map/dot_general | solution.py:69
  25.6 0.6 copy.23
  26.2 4.6 %all-to-all-start.1 = ((bf16[8,1,192]{2,1,0:T(2,128)(2,1)}), bf16[8,1,192]{2,1,0:T(2,128)(2,1)S(1)}, u32[]{:S(2)}, u32[]{:S(2)}) async-start(bf16[8,1,192]{2,1,0:T(2,128)(2,1)} %copy.23), calls=%async_computation.1 | async-start | bytes 16384 | tf_op jit(solution)/shard_map/all_to_all | solution.py:103
  30.8 0.6 dynamic_slice.7
  31.4 1.4 %fusion.9 = bf16[8,1,192]{2,0,1:T(8,128)(2,1)S(1)} fusion(bf16[8,2048]{1,0:T(8,128)(2,1)S(1)} %get-tuple-element.5, bf16[2048,192]{0,1:T(8,128)(2,1)} %param.21, f32[8]{0:T(128)S(1)} %add_rsqrt_fusion.3), kind=kOutput, calls=%fused_computation.16 | convolution fusion | flops 6294528 | bytes 822304 | tf_op jit(solution)/shard_map/dot_general | solution.py:69
  32.8 1.5 %fusion.8 = bf16[8,1,192]{2,0,1:T(8,128)(2,1)S(1)} fusion(bf16[8,2048]{1,0:T(8,128)(2,1)S(1)} %get-tuple-element.5, bf16[2048,192]{0,1:T(8,128)(2,1)} %param.22, f32[8]{0:T(128)S(1)} %add_rsqrt_fusion.3), kind=kOutput, calls=%fused_computation.15 | convolution fusion | flops 6294528 | bytes 822304 | tf_op jit(solution)/shard_map/dot_general | solution.py:69
  34.3 1.6 %fusion.16 = f32[12]{0:T(128)S(1)} fusion(bf16[2048,12]{0,1:T(8,128)(2,1)} %param.23, bf16[8,2048]{1,0:T(8,128)(2,1)S(1)} %get-tuple-element.5, s32[]{:T(128)S(6)} %select_n.9, f32[]{:T(128)} %bitcast.2), kind=kOutput, calls=%fused_computation.24 | convolution fusion | flops 49200 | bytes 57400 | tf_op jit(solution)/shard_map/dot_general | solution.py:72
  35.9 1.7 %fusion.41 = f32[12]{0:T(128)S(1)} fusion(f32[12]{0:T(128)} %param.26, bf16[2048,12]{0,1:T(8,128)(2,1)} %param.24, bf16[8,2048]{1,0:T(8,128)(2,1)S(1)} %get-tuple-element.5, s32[]{:T(128)S(6)} %select_n.9, f32[12]{0:T(128)} %param.25, f32[]{:T(128)} %bitcast.2), kind=kOutput, calls=%fused_computation.67 | convolution fusion | flops 49272 | bytes 57496 | tf_op jit(solution)/shard_map/dot_general | solution.py:72
  37.6 1.5 %fusion.11 = bf16[8,1,192]{2,0,1:T(8,128)(2,1)S(1)} fusion(bf16[8,2048]{1,0:T(8,128)(2,1)S(1)} %get-tuple-element.5, bf16[2048,192]{0,1:T(8,128)(2,1)} %param.19, f32[8]{0:T(128)S(1)} %add_rsqrt_fusion.3), kind=kOutput, calls=%fused_computation.18 | convolution fusion | flops 6294528 | bytes 822304 | tf_op jit(solution)/shard_map/dot_general | solution.py:69
  39.0 0.6 copy.24
  39.7 0.6 copy.22
  40.3 0.6 copy.25
  40.9 0.0 all-to-all-done.1
  40.9 5.1 %all-to-all-start.3 = ((bf16[8,1,192]{2,1,0:T(2,128)(2,1)}), bf16[8,1,192]{2,1,0:T(2,128)(2,1)S(1)}, u32[]{:S(2)}, u32[]{:S(2)}) async-start(bf16[8,1,192]{2,1,0:T(2,128)(2,1)} %copy.25), calls=%async_computation.3 | async-start | bytes 16384 | tf_op jit(solution)/shard_map/all_to_all | solution.py:103
  46.0 0.1 mul.181
  46.1 0.1 reduce_sum.37
  46.2 0.1 reshape.233
  46.3 0.1 fusion.64
  46.4 5.2 %all-to-all-done.3 = bf16[8,1,192]{2,1,0:T(2,128)(2,1)S(1)} async-done(((bf16[8,1,192]{2,1,0:T(2,128)(2,1)}), bf16[8,1,192]{2,1,0:T(2,128)(2,1)S(1)}, u32[]{:S(2)}, u32[]{:S(2)}) %all-to-all-start.3) | async-done | bytes 3104 | tf_op jit(solution)/shard_map/all_to_all | solution.py:103
  51.6 3.3 %all-to-all-start = ((bf16[8,1,192]{2,1,0:T(2,128)(2,1)}), bf16[8,1,192]{2,1,0:T(2,128)(2,1)S(1)}, u32[]{:S(2)}, u32[]{:S(2)}) async-start(bf16[8,1,192]{2,1,0:T(2,128)(2,1)} %copy.22), calls=%async_computation | async-start | bytes 16384 | tf_op jit(solution)/shard_map/all_to_all | solution.py:103
  54.9 0.1 broadcast_multiply_fusion.1
  55.0 5.5 %all-to-all-done = bf16[8,1,192]{2,1,0:T(2,128)(2,1)S(1)} async-done(((bf16[8,1,192]{2,1,0:T(2,128)(2,1)}), bf16[8,1,192]{2,1,0:T(2,128)(2,1)S(1)}, u32[]{:S(2)}, u32[]{:S(2)}) %all-to-all-start) | async-done | bytes 3104 | tf_op jit(solution)/shard_map/all_to_all | solution.py:103
  60.5 3.3 %all-to-all-start.2 = ((bf16[8,1,192]{2,1,0:T(2,128)(2,1)}), bf16[8,1,192]{2,1,0:T(2,128)(2,1)S(1)}, u32[]{:S(2)}, u32[]{:S(2)}) async-start(bf16[8,1,192]{2,1,0:T(2,128)(2,1)} %copy.24), calls=%async_computation.2 | async-start | bytes 16384 | tf_op jit(solution)/shard_map/all_to_all | solution.py:103
  63.8 0.0 reduce-scatter.2.cloned.1.call-start
  63.9 0.1 reshape.235
  64.0 0.1 reshape.252
  64.1 5.3 %all-to-all-done.2 = bf16[8,1,192]{2,1,0:T(2,128)(2,1)S(1)} async-done(((bf16[8,1,192]{2,1,0:T(2,128)(2,1)}), bf16[8,1,192]{2,1,0:T(2,128)(2,1)S(1)}, u32[]{:S(2)}, u32[]{:S(2)}) %all-to-all-start.2) | async-done | bytes 3104 | tf_op jit(solution)/shard_map/all_to_all | solution.py:103
  69.4 0.1 reshape.234
  69.5 0.8 fusion.34
  70.2 0.1 bitcast_multiply_fusion.2
  70.3 0.3 multiply_add_fusion
  70.6 0.0 copy-start.2
  70.6 0.5 fusion.47
  71.1 0.1 fusion.29
  71.2 0.1 fusion.32
  71.3 14.0 %all-gather.1 = bf16[8,1,1536]{2,1,0:T(2,128)(2,1)S(1)} all-gather(bf16[1,1,1536]{2,1,0:T(2,128)(2,1)S(1)} %reshape.240), channel_id=1, replica_groups=mesh['grp'=2,'dp'=2,'kv'=4,'tp'=2] {'kv','tp'}, dimensions={0}, use_global_device_ids=true | all-gather | bytes 27648 | tf_op jit(solution)/shard_map/all_gather | solution.py:110
  85.3 0.0 copy-done
  85.3 0.2 fusion.7
  85.5 14.1 %all-gather = bf16[64,256]{1,0:T(8,128)(2,1)S(1)} all-gather(bf16[8,256]{1,0:T(8,128)(2,1)S(1)} %fusion.7), channel_id=2, replica_groups=mesh['grp'=2,'dp'=2,'kv'=4,'tp'=2] {'kv','tp'}, dimensions={0}, use_global_device_ids=true | all-gather | bytes 36864 | tf_op jit(solution)/shard_map/all_gather | solution.py:119
  99.6 0.1 multiply_reduce_fusion
  99.8 0.0 copy-done.4
  99.8 5.3 %convolution_convert_fusion = bf16[8,2048]{1,0:T(8,128)(2,1)} fusion(bf16[1024,2048]{1,0:T(8,128)(2,1)} %param.31, bf16[2048,1024]{1,0:T(8,128)(2,1)} %param.30, f32[8,2048]{1,0:T(8,128)S(1)} %bitcast.87, f32[2048]{0:T(1024)S(1)} %copy-done.4, f32[8]{0:T(128)S(1)} %add_rsqrt_fusion), kind=kOutput, calls=%fused_computation | convolution fusion | flops 67190784 | bytes 8495136 | tf_op jit(solution)/shard_map/dot_general | solution.py:127
  105.1 0.0 reduce-scatter.2.cloned.1.call-update
  105.1 28.9 %reduce-scatter.2.cloned.1.call-done = bf16[8,256]{1,0:T(8,128)(2,1)} async-done(((bf16[8,2048]{1,0:T(8,128)(2,1)}), bf16[8,256]{1,0:T(8,128)(2,1)}) %reduce-scatter.2.cloned.1.call-update) | async-done | bytes 4112 | tf_op jit(solution)/shard_map/reduce_scatter | solution.py:128
  134.0 1.3 add_convert_fusion
  (18 shorter events, 0.2 us)
Async XLA Ops:
  7.2 78.2 %copy-start = (bf16[1536,256]{1,0:T(8,128)(2,1)S(1)}, bf16[1536,256]{1,0:T(8,128)(2,1)}, u32[]{:S(2)}) copy-start(bf16[1536,256]{1,0:T(8,128)(2,1)} %param.28) | copy-start | bytes 2359300
  7.2 78.2 %copy-start.3 = (bf16[8,256]{1,0:T(8,128)(2,1)S(1)}, bf16[8,256]{1,0:T(8,128)(2,1)}, u32[]{:S(2)}) copy-start(bf16[8,256]{1,0:T(8,128)(2,1)} %param.16) | copy-start | bytes 12292
  7.2 62.3 %copy-start.1 = (f32[1,12,16384]{2,0,1:T(1,128)S(1)}, f32[1,12,16384]{2,0,1:T(1,128)}, u32[]{:S(2)}) copy-start(f32[1,12,16384]{2,0,1:T(1,128)} %param.17) | copy-start | bytes 2359300
  7.2 64.0 %copy-start.5 = (f32[128]{0:T(128)S(1)}, f32[128]{0:T(128)}, u32[]{:S(2)}) copy-start(f32[128]{0:T(128)} %param.27) | copy-start | bytes 1540
  7.2 92.6 %copy-start.4 = (f32[2048]{0:T(1024)S(1)}, f32[2048]{0:T(1024)}, u32[]{:S(2)}) copy-start(f32[2048]{0:T(1024)} %param.29) | copy-start | bytes 24580
  26.2 14.7 %all-to-all-start.1 = ((bf16[8,1,192]{2,1,0:T(2,128)(2,1)}), bf16[8,1,192]{2,1,0:T(2,128)(2,1)S(1)}, u32[]{:S(2)}, u32[]{:S(2)}) async-start(bf16[8,1,192]{2,1,0:T(2,128)(2,1)} %copy.23), calls=%async_computation.1 | async-start | bytes 16384 | tf_op jit(solution)/shard_map/all_to_all | solution.py:103
  40.9 10.7 %all-to-all-start.3 = ((bf16[8,1,192]{2,1,0:T(2,128)(2,1)}), bf16[8,1,192]{2,1,0:T(2,128)(2,1)S(1)}, u32[]{:S(2)}, u32[]{:S(2)}) async-start(bf16[8,1,192]{2,1,0:T(2,128)(2,1)} %copy.25), calls=%async_computation.3 | async-start | bytes 16384 | tf_op jit(solution)/shard_map/all_to_all | solution.py:103
  51.6 8.9 %all-to-all-start = ((bf16[8,1,192]{2,1,0:T(2,128)(2,1)}), bf16[8,1,192]{2,1,0:T(2,128)(2,1)S(1)}, u32[]{:S(2)}, u32[]{:S(2)}) async-start(bf16[8,1,192]{2,1,0:T(2,128)(2,1)} %copy.22), calls=%async_computation | async-start | bytes 16384 | tf_op jit(solution)/shard_map/all_to_all | solution.py:103
  60.5 8.9 %all-to-all-start.2 = ((bf16[8,1,192]{2,1,0:T(2,128)(2,1)}), bf16[8,1,192]{2,1,0:T(2,128)(2,1)S(1)}, u32[]{:S(2)}, u32[]{:S(2)}) async-start(bf16[8,1,192]{2,1,0:T(2,128)(2,1)} %copy.24), calls=%async_computation.2 | async-start | bytes 16384 | tf_op jit(solution)/shard_map/all_to_all | solution.py:103
  63.8 70.2 %reduce-scatter.2.cloned.1.call-start = ((), (), s32[]{:S(2)}) async-start(), calls=%async_computation.5 | async-start | bytes 36864 | tf_op jit(solution)/shard_map/reduce_scatter | solution.py:128
  70.6 34.5 %copy-start.2 = (f32[12,128,128]{2,1,0:T(8,128)}, f32[12,128,128]{2,1,0:T(8,128)S(1)}, u32[]{:S(2)}) copy-start(f32[12,128,128]{2,1,0:T(8,128)S(1)} %multiply_add_fusion) | copy-start | bytes 2359300
Sparse Core Ops, SparseCore 0:
  105.2 28.7 reduce-scatter.1
